TPU v7x, 32 devices: a whole 2x2x4 slice. The times are simulated.
32 devices in a mesh: sp: 8 (over z, x), tp: 4 (over y, core).
Axes of the slice: x: 2, y: 2, z: 4, core: 2. Of those that a mesh axis runs over, the one named last changes fastest.
Arguments:
- latents: bfloat16 [4096, 2048], P(('sp', 'tp')), may hold values from -6 to 6
- context: bfloat16 [512, 2048], P('sp'), may hold values from -6 to 6
- cond: float32 [2048], P('sp'), may hold values from -6 to 6
- ctx_cond: float32 [2048], P('sp'), may hold values from -6 to 6
- mod_weight: float32 [2048, 6144], P('sp', 'tp'), may hold values from -0.125 to 0.125
- query_weight: bfloat16 [2048, 2048], P(None, 'tp'), may hold values from -1 to 1, as said below
- key_matrix: bfloat16 [2048, 1024], P(None, 'tp'), may hold values from -1 to 1, as said below
- value_matrix: bfloat16 [2048, 1024], P(None, 'tp'), may hold values from -0.125 to 0.125
- out_weight: bfloat16 [2048, 2048], P('tp'), may hold values from -0.125 to 0.125
- query_gain: float32 [128], replicated, may hold values from 0.7 to 7
- key_gain: float32 [128], replicated, may hold values from 0.7 to 7
Outputs:
- updated: bfloat16 [4096, 2048], P(('sp', 'tp'))
Inputs may be any that keep to these rules, and one draw needn't show every extreme that they name: `query_weight`: entries of order 2048 to the power -1/2. `key_matrix`: entries of order 2048 to the power -1/2.
All inputs are finite; a program needn't handle non-finite values.
Results may differ from a plain program's by a relative error of at most 0.0085.
The roundings to bfloat16 on the way count: a program that leaves them out, or rounds other values in their place, can miss the bound.
Values may be sent and summed in bfloat16 or wider, within the bound.
A program may use at most 128 MiB of HBM per device.

v0:
```python
import math
import jax
import jax.numpy as jnp
from jax import lax
from jax.sharding import PartitionSpec as P

GRID_W = 64
NORM_EPS = 1e-06
ROPE_BASE = 10000.0


def normalize(latent_value_rows):
    return latent_value_rows * lax.rsqrt(
        jnp.mean(latent_value_rows * latent_value_rows, axis=-1, keepdims=True) + NORM_EPS
    )


def rotate(latent_value_rows, positions):
    quarter = latent_value_rows.shape[-1] // 2
    inv_freq = ROPE_BASE ** (-jnp.arange(quarter, dtype=jnp.float32) / quarter)
    angles = positions.astype(jnp.float32)[:, None] * inv_freq[None, :]
    cos_table = jnp.cos(angles)[:, None, :]
    sin_table = jnp.sin(angles)[:, None, :]
    first, second = (latent_value_rows[..., :quarter], latent_value_rows[..., quarter:])
    return jnp.concatenate(
        [first * cos_table - second * sin_table, second * cos_table + first * sin_table], axis=-1
    )


def axial(latent_value_rows, positions):
    half_dim = latent_value_rows.shape[-1] // 2
    return jnp.concatenate(
        [
            rotate(latent_value_rows[..., :half_dim], positions // GRID_W),
            rotate(latent_value_rows[..., half_dim:], positions % GRID_W),
        ],
        axis=-1,
    )


def modulate(latent_value_rows, mod_row):
    model_width = latent_value_rows.shape[-1]
    shift_vec = mod_row[:model_width]
    scale_vec = mod_row[model_width : 2 * model_width]
    return (
        normalize(latent_value_rows.astype(jnp.float32)) * (1.0 + scale_vec) + shift_vec
    ).astype(jnp.bfloat16)


def body(
    latents,
    context,
    cond,
    ctx_cond,
    mod_weight,
    query_weight,
    key_matrix,
    value_matrix,
    out_weight,
    query_gain,
    key_gain,
):
    model_width = latents.shape[1]
    head_dim = query_gain.shape[0]
    sp_count = lax.axis_size("sp")
    partials = jnp.dot(
        jax.nn.silu(jnp.stack([cond, ctx_cond])), mod_weight, precision=lax.Precision.HIGHEST
    )
    summed = lax.psum(partials, "sp")
    modulation = lax.all_gather(summed, "tp", axis=1, tiled=True)
    gate_vec = modulation[0, 2 * model_width :]
    normalised_rows = modulate(latents, modulation[0])
    prefix_normalised = modulate(context, modulation[1])
    query_cols = query_weight.shape[1]
    key_cols = key_matrix.shape[1]
    piece = lax.all_gather(normalised_rows, "tp", axis=0, tiled=True)
    projected = jnp.concatenate(
        [
            jnp.dot(piece, query_weight, preferred_element_type=jnp.float32),
            jnp.dot(piece, key_matrix, preferred_element_type=jnp.float32),
            jnp.dot(piece, value_matrix, preferred_element_type=jnp.float32),
        ],
        axis=1,
    )
    row_count = projected.shape[0]
    positions = lax.axis_index("sp") * row_count + jnp.arange(row_count, dtype=jnp.int32)
    query_heads = projected[:, :query_cols].reshape(row_count, -1, head_dim)
    query_heads = axial(normalize(query_heads) * query_gain, positions).astype(jnp.bfloat16)
    key_heads = projected[:, query_cols : query_cols + key_cols].reshape(row_count, -1, head_dim)
    key_heads = axial(normalize(key_heads) * key_gain, positions).astype(jnp.bfloat16)
    value_heads = (
        projected[:, query_cols + key_cols :].reshape(row_count, -1, head_dim).astype(jnp.bfloat16)
    )
    key_part = jnp.dot(prefix_normalised, key_matrix, preferred_element_type=jnp.float32).reshape(
        prefix_normalised.shape[0], -1, head_dim
    )
    value_part = jnp.dot(
        prefix_normalised, value_matrix, preferred_element_type=jnp.float32
    ).reshape(prefix_normalised.shape[0], -1, head_dim)
    local_keys = (normalize(key_part) * key_gain).astype(jnp.bfloat16)
    local_values = value_part.astype(jnp.bfloat16)
    prefix_keys, prefix_values = (
        lax.all_gather(local_keys, "sp", axis=0, tiled=True),
        lax.all_gather(local_values, "sp", axis=0, tiled=True),
    )
    kv_local = key_heads.shape[1]
    group_size = query_heads.shape[1] // kv_local
    grouped = query_heads.reshape(row_count, kv_local, group_size, head_dim).transpose(1, 2, 0, 3)
    grouped = grouped.reshape(kv_local, group_size * row_count, head_dim)
    inv_root = head_dim ** (-0.5)
    lift = math.log(sp_count * row_count / (2.0 * prefix_keys.shape[0]))
    ctx_scores = (
        jnp.einsum("hqd,khd->hqk", grouped, prefix_keys, preferred_element_type=jnp.float32)
        * inv_root
        + lift
    )
    top_init = jnp.max(ctx_scores, axis=-1)
    ctx_weights = jnp.exp(ctx_scores - top_init[..., None])
    initial = (
        top_init,
        jnp.sum(ctx_weights, axis=-1),
        jnp.einsum(
            "hqk,khd->hqd",
            ctx_weights.astype(jnp.bfloat16),
            prefix_values,
            preferred_element_type=jnp.float32,
        ),
    )

    def update(state_now, key_block, value_block):
        top_old, total_old, acc_old = state_now
        scores = (
            jnp.einsum("hqd,khd->hqk", grouped, key_block, preferred_element_type=jnp.float32)
            * inv_root
        )
        top_new = jnp.maximum(top_old, jnp.max(scores, axis=-1))
        factor = jnp.exp(top_old - top_new)
        weights_now = jnp.exp(scores - top_new[..., None])
        acc_new = acc_old * factor[..., None] + jnp.einsum(
            "hqk,khd->hqd",
            weights_now.astype(jnp.bfloat16),
            value_block,
            preferred_element_type=jnp.float32,
        )
        return (top_new, total_old * factor + jnp.sum(weights_now, axis=-1), acc_new)

    key_piece = lax.all_gather(key_heads, "sp", axis=0, tiled=True)
    value_piece = lax.all_gather(value_heads, "sp", axis=0, tiled=True)
    key_count = key_piece.shape[0]
    rows_per_block = math.gcd(key_count, 2048)
    block_count = key_count // rows_per_block
    key_blocks = key_piece.reshape(block_count, rows_per_block, kv_local, head_dim)
    value_blocks = value_piece.reshape(block_count, rows_per_block, kv_local, head_dim)

    def one_step(state_in, blocks_in):
        return (update(state_in, blocks_in[0], blocks_in[1]), None)

    state_out, _ = lax.scan(one_step, initial, (key_blocks, value_blocks))
    top_fin, total_fin, acc_fin = state_out
    attended = (acc_fin / total_fin[..., None]).astype(jnp.bfloat16)
    attended = (
        attended.reshape(kv_local, group_size, row_count, head_dim)
        .transpose(2, 0, 1, 3)
        .reshape(row_count, -1)
    )
    mixed_rows = lax.psum_scatter(
        jnp.dot(attended, out_weight, preferred_element_type=jnp.float32).astype(jnp.bfloat16),
        "tp",
        scatter_dimension=0,
        tiled=True,
    ).astype(jnp.float32)
    return (latents.astype(jnp.float32) + gate_vec * normalize(mixed_rows)).astype(jnp.bfloat16)


def solution(mesh):
    placed = (
        P(("sp", "tp"), None),
        P("sp", None),
        P("sp"),
        P("sp"),
        P("sp", "tp"),
        P(None, "tp"),
        P(None, "tp"),
        P(None, "tp"),
        P("tp", None),
        P(),
        P(),
    )
    return jax.shard_map(
        body, mesh=mesh, in_specs=placed, out_specs=P(("sp", "tp"), None), check_vma=False
    )
```

profile of v0, /device:TPU:0, one launch (start us, length us, event | category | flops | bytes accessed | tf_op | source)
XLA Modules:
  0.0 286.1 jit_solution(9915169423210026204)
XLA Ops:
  6.5 2.4 fusion.41
  9.0 38.8 %psum.7 = f32[2,1536]{1,0:T(2,128)S(1)} all-reduce(f32[2,1536]{1,0:T(2,128)S(1)} %fusion.41), channel_id=1, replica_groups=mesh['sp'=8,'tp'=4] {'sp'}, use_global_device_ids=true, to_apply=%region_0.1 | all-reduce | flops 3072 | bytes 24576 | tf_op jit(solution)/shard_map/psum | solution.py:69
  47.8 5.2 %all_gather.18 = f32[2,6144]{1,0:T(2,128)S(1)} all-gather(f32[2,1536]{1,0:T(2,128)S(1)} %psum.7), channel_id=1, replica_groups=mesh['sp'=8,'tp'=4] {'tp'}, dimensions={1}, use_global_device_ids=true | all-gather | bytes 61440 | tf_op jit(solution)/shard_map/all_gather | solution.py:70
  53.6 1.2 fusion.27
  54.9 2.1 fusion.30
  57.9 0.9 copy.83
  58.7 0.9 copy.84
  59.6 17.4 %all-gather.4.cloned.1.call-done = bf16[512,2048]{1,0:T(8,128)(2,1)} async-done(((bf16[128,2048]{1,0:T(8,128)(2,1)}), bf16[512,2048]{1,0:T(8,128)(2,1)}) %all-gather.4.cloned.1.call-update) | async-done | bytes 2097168 | tf_op jit(solution)/shard_map/all_gather | solution.py:76
  77.0 4.0 %multiply_reduce_fusion.1 = (f32[512,2]{0,1:T(2,128)}, f32[512,256]{0,1:T(8,128)}) fusion(bf16[512,2048]{1,0:T(8,128)(2,1)} %all-gather.4.cloned.1.call-done, bf16[2048,256]{1,0:T(8,128)(2,1)} %param.19), kind=kOutput, calls=%fused_computation.57 | convolution fusion | flops 537132032 | bytes 3674112 | tf_op jit(solution)/shard_map/dot_general | solution.py:80
  81.0 1.3 copy.80
  82.3 0.7 add_rsqrt_fusion.1
  83.0 0.9 multiply_multiply_fusion.1
  83.8 1.5 subtract_convert_fusion.1
  85.4 1.1 pad_maximum_fusion.1
  86.5 0.7 fusion.32
  87.3 3.3 %convolution_convert_fusion.1 = bf16[512,256]{0,1:T(8,128)(2,1)} fusion(bf16[512,2048]{1,0:T(8,128)(2,1)} %all-gather.4.cloned.1.call-done, bf16[2048,256]{1,0:T(8,128)(2,1)} %param.20), kind=kOutput, calls=%fused_computation.32 | convolution fusion | flops 537001984 | bytes 3407872 | tf_op jit(solution)/shard_map/dot_general | solution.py:81
  90.6 1.8 copy.85
  92.5 0.7 add_rsqrt_fusion.4
  93.7 1.0 fusion.39
  94.7 0.9 reshape.233
  95.8 1.6 fusion.24
  97.4 0.9 fusion.37
  98.4 31.6 %all_gather.20 = bf16[512,2,128]{2,0,1:T(8,128)(2,1)S(1)} all-gather(bf16[64,2,128]{2,0,1:T(8,128)(2,1)S(1)} %fusion.37), channel_id=1, replica_groups=mesh['sp'=8,'tp'=4] {'sp'}, dimensions={0}, use_global_device_ids=true | all-gather | bytes 294912 | tf_op jit(solution)/shard_map/all_gather | solution.py:103
  129.9 33.5 %all_gather.21 = bf16[512,2,128]{2,0,1:T(8,128)(2,1)} all-gather(bf16[64,2,128]{2,0,1:T(8,128)(2,1)S(1)} %bitcast.103), channel_id=1, replica_groups=mesh['sp'=8,'tp'=4] {'sp'}, dimensions={0}, use_global_device_ids=true | all-gather | bytes 294912 | tf_op jit(solution)/shard_map/all_gather | solution.py:104
  163.5 3.6 %multiply_reduce_fusion = (f32[512,4]{0,1:T(4,128)S(1)}, f32[512,512]{0,1:T(8,128)S(1)}) fusion(bf16[512,2048]{1,0:T(8,128)(2,1)} %all-gather.4.cloned.1.call-done, bf16[2048,512]{1,0:T(8,128)(2,1)} %param.18), kind=kOutput, calls=%fused_computation.44 | convolution fusion | flops 1074264064 | bytes 5251072 | tf_op jit(solution)/shard_map/dot_general | solution.py:79
  167.3 0.9 subtract_convert_fusion.3
  168.5 1.2 copy.73
  169.6 1.9 copy.74
  171.5 1.9 copy.75
  173.5 1.9 pad_maximum_fusion
  175.3 0.8 copy-done.1
  176.1 0.7 fusion.16
  176.9 0.8 fusion.18
  177.7 1.2 fusion.19
  179.0 10.1 %all-gather.8.cloned.1.call-done = bf16[4096,2,128]{2,0,1:T(8,128)(2,1)} async-done(((bf16[512,2,128]{2,0,1:T(8,128)(2,1)}), bf16[4096,2,128]{2,0,1:T(8,128)(2,1)}) %all-gather.8.cloned.1.call-update) | async-done | bytes 2097168 | tf_op jit(solution)/shard_map/all_gather | solution.py:148
  189.1 52.1 %while.14 = (s32[]{:T(128)}, f32[2,1024]{1,0:T(2,128)S(1)}, f32[2,1024]{1,0:T(2,128)S(1)}, f32[2,1024,128]{2,1,0:T(8,128)S(1)}, bf16[2,2048,2,128]{3,1,0,2:T(8,1...) while((s32[]{:T(128)}, f32[2,1024]{1,0:T(2,128)S(1)}, ...), condition=%wide.region_11.12_spmd, body=%wide.region_8.11_spmd.sunk | while | flops 2181566464 | bytes 55182420 | solution.py:158
  189.1 9.4 %bitcast_reduce_fusion.2 = (f32[2,1024]{1,0:T(2,128)S(1)}, f32[2,2048,1024]{2,1,0:T(8,128)}) fusion(bf16[2,1024,128]{2,1,0:T(8,128)(2,1)} %get-tuple-element.194, bf16[2,2048,2,128]{3,1,0,2:T(8,128)(2,1)} %get-tuple-element.193, s32[]{:T(128)} %get-tuple-element.181), kind=kOutput, calls=%fused_computation.1.clone.1 | convolution fusion | flops 1082128384 | bytes 18358784 | tf_op jit(solution)/shard_map/while/body/eval_jaxpr/hqd,khd->hqk/dot_general | solution.py:133
  198.5 8.5 %fusion.80 = f32[2,1024]{1,0:T(2,128)S(1)} fusion(f32[2,2048,1024]{2,1,0:T(8,128)} %get-tuple-element.170, f32[2,1024]{1,0:T(2,128)S(1)} %max.4), kind=kLoop, calls=%fused_computation.4.clone.1 | loop fusion | flops 12580864 | bytes 16793600 | tf_op jit(solution)/shard_map/while/body/eval_jaxpr/reduce_sum | solution.py:145
  207.0 8.1 %fusion.81 = f32[2,1024,128]{2,1,0:T(8,128)S(1)} fusion(f32[2,2048,1024]{2,1,0:T(8,128)} %get-tuple-element.170, f32[2,1024]{1,0:T(2,128)S(1)} %max.4, bf16[2,2048,2,128]{3,1,0,2:T(8,128)(2,1)} %get-tuple-element.195, s32[]{:T(128)} %get-tuple-element.181, f32[2,1024,128]{2,1,0:T(8,128)S(1)} %get-tuple-element.184, f32[2,1024]{1,0:T(2,128)S(1)} %get-tuple-element.172), kind=kOutput, calls=%fused_computation.6.clone.1 | convolution fusion | flops 1086849024 | bytes 19939840 | tf_op jit(solution)/shard_map/while/body/eval_jaxpr/hqk,khd->hqd/dot_general | solution.py:139
  215.1 9.4 %bitcast_reduce_fusion.2 = (f32[2,1024]{1,0:T(2,128)S(1)}, f32[2,2048,1024]{2,1,0:T(8,128)}) fusion(bf16[2,1024,128]{2,1,0:T(8,128)(2,1)} %get-tuple-element.194, bf16[2,2048,2,128]{3,1,0,2:T(8,128)(2,1)} %get-tuple-element.193, s32[]{:T(128)} %get-tuple-element.181), kind=kOutput, calls=%fused_computation.1.clone.1 | convolution fusion | flops 1082128384 | bytes 18358784 | tf_op jit(solution)/shard_map/while/body/eval_jaxpr/hqd,khd->hqk/dot_general | solution.py:133
  224.5 8.5 %fusion.80 = f32[2,1024]{1,0:T(2,128)S(1)} fusion(f32[2,2048,1024]{2,1,0:T(8,128)} %get-tuple-element.170, f32[2,1024]{1,0:T(2,128)S(1)} %max.4), kind=kLoop, calls=%fused_computation.4.clone.1 | loop fusion | flops 12580864 | bytes 16793600 | tf_op jit(solution)/shard_map/while/body/eval_jaxpr/reduce_sum | solution.py:145
  233.1 8.1 %fusion.81 = f32[2,1024,128]{2,1,0:T(8,128)S(1)} fusion(f32[2,2048,1024]{2,1,0:T(8,128)} %get-tuple-element.170, f32[2,1024]{1,0:T(2,128)S(1)} %max.4, bf16[2,2048,2,128]{3,1,0,2:T(8,128)(2,1)} %get-tuple-element.195, s32[]{:T(128)} %get-tuple-element.181, f32[2,1024,128]{2,1,0:T(8,128)S(1)} %get-tuple-element.184, f32[2,1024]{1,0:T(2,128)S(1)} %get-tuple-element.172), kind=kOutput, calls=%fused_computation.6.clone.1 | convolution fusion | flops 1086849024 | bytes 19939840 | tf_op jit(solution)/shard_map/while/body/eval_jaxpr/hqk,khd->hqd/dot_general | solution.py:139
  241.2 1.1 divide_convert_fusion
  242.3 1.2 copy.88
  243.6 2.6 convolution_convert_fusion
  246.3 29.9 %reduce-scatter.2.cloned.1.call-done = bf16[128,2048]{1,0:T(8,128)(2,1)} async-done(((bf16[512,2048]{1,0:T(8,128)(2,1)}), bf16[128,2048]{1,0:T(8,128)(2,1)}) %reduce-scatter.2.cloned.1.call-update) | async-done | bytes 524304 | tf_op jit(solution)/shard_map/reduce_scatter | solution.py:166
  276.2 1.2 fusion.25
  277.4 2.1 fusion.31
  (55 shorter events, 3.0 us)
Async XLA Ops:
  6.5 237.1 %copy-start = (bf16[512,2048]{1,0:T(8,128)(2,1)S(1)}, bf16[512,2048]{1,0:T(8,128)(2,1)}, u32[]{:S(2)}) copy-start(bf16[512,2048]{1,0:T(8,128)(2,1)} %param.21) | copy-start | bytes 6291460
  6.5 70.5 %all-gather.4.cloned.1.call-start = ((), (), s32[]{:S(2)}) async-start(), calls=%async_computation.1 | async-start | bytes 2621440 | tf_op jit(solution)/shard_map/all_gather | solution.py:76
  57.0 122.0 %all-gather.6.cloned.1.call-start = ((), (), s32[]{:S(2)}) async-start(), calls=%async_computation.2 | async-start | bytes 2359296 | tf_op jit(solution)/shard_map/all_gather | solution.py:147
  57.6 19.4 %copy-start.6 = (f32[512,32]{0,1:T(8,128)}, f32[512,32]{0,1:T(8,128)S(1)}, u32[]{:S(2)}) copy-start(f32[512,32]{0,1:T(8,128)S(1)} %get-tuple-element.112) | copy-start | bytes 196612
  57.6 19.4 %copy-start.8 = (f32[512,32]{0,1:T(8,128)}, f32[512,32]{0,1:T(8,128)S(1)}, u32[]{:S(2)}) copy-start(f32[512,32]{0,1:T(8,128)S(1)} %get-tuple-element.113) | copy-start | bytes 196612
  81.0 5.5 %copy-start.3 = (bf16[64,2048]{1,0:T(8,128)(2,1)S(1)}, bf16[64,2048]{1,0:T(8,128)(2,1)}, u32[]{:S(2)}) copy-start(bf16[64,2048]{1,0:T(8,128)(2,1)} %param.14) | copy-start | bytes 786436
  85.3 8.4 %copy-start.4 = (bf16[2048,256]{1,0:T(8,128)(2,1)S(1)}, bf16[2048,256]{1,0:T(8,128)(2,1)}, u32[]{:S(2)}) copy-start(bf16[2048,256]{1,0:T(8,128)(2,1)} %param.19) | copy-start | bytes 3145732
  86.5 102.6 %all-gather.8.cloned.1.call-start = ((), (), s32[]{:S(2)}) async-start(), calls=%async_computation.3 | async-start | bytes 2359296 | tf_op jit(solution)/shard_map/all_gather | solution.py:148
  92.4 183.8 %reduce-scatter.2.cloned.1.call-start = ((), (), s32[]{:S(2)}) async-start(), calls=%async_computation.4 | async-start | bytes 2621440 | tf_op jit(solution)/shard_map/reduce_scatter | solution.py:166
  93.1 0.6 copy-start.11
  163.4 3.6 %copy-start.12 = (f32[128]{0:T(128)S(1)}, f32[128]{0:T(128)}, u32[]{:S(2)}) copy-start(f32[128]{0:T(128)} %param.22) | copy-start | bytes 1540
  163.4 3.8 %copy-start.7 = (f32[512,32]{0,1:T(8,128)S(1)}, f32[512,32]{0,1:T(8,128)}, u32[]{:S(2)}) copy-start(f32[512,32]{0,1:T(8,128)} %copy-done.6) | copy-start | bytes 196612
  163.4 3.8 %copy-start.9 = (f32[512,32]{0,1:T(8,128)S(1)}, f32[512,32]{0,1:T(8,128)}, u32[]{:S(2)}) copy-start(f32[512,32]{0,1:T(8,128)} %copy-done.8) | copy-start | bytes 196612
  175.3 0.8 copy-start.1
  176.1 1.6 copy-start.5
  243.6 33.8 %copy-start.2 = (bf16[128,2048]{1,0:T(8,128)(2,1)S(1)}, bf16[128,2048]{1,0:T(8,128)(2,1)}, u32[]{:S(2)}) copy-start(bf16[128,2048]{1,0:T(8,128)(2,1)} %param.13) | copy-start | bytes 1572868
  243.6 33.8 %copy-start.10 = (f32[1,2048]{1,0:T(1,128)S(1)}, f32[1,2048]{1,0:T(1,128)}, u32[]{:S(2)}) copy-start(f32[1,2048]{1,0:T(1,128)} %get-tuple-element.103) | copy-start | bytes 24580
Sparse Core Ops, SparseCore 0:
  57.1 19.8 all-gather.3
  86.6 52.3 all-gather.5
  141.2 47.7 all-gather.7
  246.4 29.7 reduce-scatter.1
where the time goes:
time: 287 us; the launch traced here: 286 us
  blocking collectives  109 us (38%)
  waiting for transfers between devices  57.5 us (20%)
  matrix products  55.5 us (19%)
  other arithmetic  36.5 us (13%)
  local copies, waits for them, and re-layouts  13.9 us (5%)
  between operations  13.4 us (5%)
    psum x1, blocking collectives, body(): summed = lax.psum(partials, 'sp')  38.8 us
    all_gather x1, blocking collectives, body(): lax.all_gather(local_values, 'sp', axis=0, tiled=True)  33.5 us
    all_gather x1, blocking collectives, body(): lax.all_gather(local_keys, 'sp', axis=0, tiled=True)  31.6 us
    reduce_scatter x1, waiting for transfers between devices, body(): lax.psum_scatter(jnp.dot(attended, out_weight, preferred_element_type=jnp...  29.9 us
    dot_general x2, matrix products, update(): jnp.einsum('hqd,khd->hqk', grouped, key_block, preferred_element_type=jnp...  18.8 us
    all_gather x1, waiting for transfers between devices, body(): piece = lax.all_gather(normalised_rows, 'tp', axis=0, tiled=True)  17.4 us
    reduce_sum x2, other arithmetic, update(): jnp.sum(weights_now, axis=-1)  17 us
    dot_general x2, matrix products, update(): jnp.einsum('hqk,khd->hqd', weights_now.astype(jnp.bfloat16), value_block,...  16.2 us
  transfers between devices with their start and end apart: 4, of which 3 were waited for; matrix products, arithmetic and copies ran while one was open for 10% of the time, Pallas kernels for 0%

commit v1 on v0

--- a/solution.py
+++ b/solution.py
@@ -66,7 +66,9 @@
     partials = jnp.dot(
         jax.nn.silu(jnp.stack([cond, ctx_cond])), mod_weight, precision=lax.Precision.HIGHEST
     )
-    summed = lax.psum(partials, "sp")
+    summed = partials
+    for hop in (1, 2, 4):
+        summed = summed + lax.ppermute(summed, "sp", [(dev, dev ^ hop) for dev in range(8)])
     modulation = lax.all_gather(summed, "tp", axis=1, tiled=True)
     gate_vec = modulation[0, 2 * model_width :]
     normalised_rows = modulate(latents, modulation[0])

time: 287 us -> 265 us (0.923)
  blocking collectives: 109 us -> 70.7 us
  starting transfers between devices: 0.13 us -> 8.38 us
  waiting for transfers between devices: 57.5 us -> 64.8 us
    psum x1 -> x0, blocking collectives: 38.8 us -> none  [body(): summed = lax.psum(partials, 'sp')]
    ppermute x0 -> x3, starting transfers between devices: none -> 8.25 us  [body(): lax.ppermute(summed, 'sp', [(dev, dev ^ hop) for dev in range(8)])]
    all_gather x1, waiting for transfers between devices: 17.4 us -> 21.7 us  [body(): piece = lax.all_gather(normalised_rows, 'tp', axis=0, tiled=True)]
    ppermute x0 -> x3, waiting for transfers between devices: none -> 3.79 us  [body(): lax.ppermute(summed, 'sp', [(dev, dev ^ hop) for dev in range(8)])]
  transfers between devices with their start and end apart: 4 -> 7, of which waited for: 3 -> 6; matrix products, arithmetic and copies ran while one was open for 10% -> 12% of each run, Pallas kernels for 0% -> 0%
where the time goes in v1:
time: 265 us; the launch traced here: 264 us
  blocking collectives  70.7 us (27%)
  waiting for transfers between devices  64.8 us (24%)
  matrix products  56.1 us (21%)
  other arithmetic  37 us (14%)
  between operations  13.4 us (5%)
  local copies, waits for them, and re-layouts  13.3 us (5%)
  starting transfers between devices  8.38 us (3%)
    all_gather x1, blocking collectives, body(): lax.all_gather(local_values, 'sp', axis=0, tiled=True)  33.7 us
    all_gather x1, blocking collectives, body(): lax.all_gather(local_keys, 'sp', axis=0, tiled=True)  31.9 us
    reduce_scatter x1, waiting for transfers between devices, body(): lax.psum_scatter(jnp.dot(attended, out_weight, preferred_element_type=jnp...  29.8 us
    all_gather x1, waiting for transfers between devices, body(): piece = lax.all_gather(normalised_rows, 'tp', axis=0, tiled=True)  21.7 us
    dot_general x2, matrix products, update(): jnp.einsum('hqd,khd->hqk', grouped, key_block, preferred_element_type=jnp...  18.8 us
    reduce_sum x2, other arithmetic, update(): jnp.sum(weights_now, axis=-1)  17 us
    dot_general x2, matrix products, update(): jnp.einsum('hqk,khd->hqd', weights_now.astype(jnp.bfloat16), value_block,...  16.2 us
    all_gather x1, waiting for transfers between devices, body(): value_piece = lax.all_gather(value_heads, 'sp', axis=0, tiled=True)  9.34 us
  transfers between devices with their start and end apart: 7, of which 6 were waited for; matrix products, arithmetic and copies ran while one was open for 12% of the time, Pallas kernels for 0%

profile of v1, /device:TPU:0, one launch (start us, length us, event | category | flops | bytes accessed | tf_op | source)
XLA Modules:
  0.0 263.9 jit_solution(15910089554831076522)
XLA Ops:
  6.5 2.4 fusion.41
  9.0 3.0 %collective-permute-start = (f32[2,1536]{1,0:T(2,128)S(1)}, f32[2,1536]{1,0:T(2,128)S(1)}, u32[]{:S(2)}, u32[]{:S(2)}) collective-permute-start(f32[2,1536]{1,0:T(2,128)S(1)} %fusion.41), channel_id=1, source_target_pairs={{0,4},{4,0},{8,12},{12,8},{16,20},{20,16},{24,28},{28,24},{1,5},{5... | collective-permute-start | bytes 36872 | tf_op jit(solution)/shard_map/ppermute | solution.py:71
  12.0 1.7 collective-permute-done
  13.7 2.2 collective-permute-start.1
  15.8 1.2 fusion.27
  17.5 3.1 %collective-permute-start.2 = (f32[2,1536]{1,0:T(2,128)S(1)}, f32[2,1536]{1,0:T(2,128)S(1)}, u32[]{:S(2)}, u32[]{:S(2)}) collective-permute-start(f32[2,1536]{1,0:T(2,128)S(1)} %add.165), channel_id=1, source_target_pairs={{0,16},{4,20},{8,24},{12,28},{16,0},{20,4},{24,8},{28,12},{1,17},{... | collective-permute-start | bytes 36872 | tf_op jit(solution)/shard_map/ppermute | solution.py:71
  20.6 1.7 collective-permute-done.2
  22.3 5.2 %all_gather.18 = f32[2,6144]{1,0:T(2,128)S(1)} all-gather(f32[2,1536]{1,0:T(2,128)S(1)} %add.166), channel_id=1, replica_groups=mesh['sp'=8,'tp'=4] {'tp'}, dimensions={1}, use_global_device_ids=true | all-gather | bytes 61440 | tf_op jit(solution)/shard_map/all_gather | solution.py:72
  28.1 2.1 fusion.30
  31.1 0.8 copy.83
  32.0 0.8 copy.84
  32.8 21.7 %all-gather.4.cloned.1.call-done = bf16[512,2048]{1,0:T(8,128)(2,1)} async-done(((bf16[128,2048]{1,0:T(8,128)(2,1)}), bf16[512,2048]{1,0:T(8,128)(2,1)}) %all-gather.4.cloned.1.call-update) | async-done | bytes 2097168 | tf_op jit(solution)/shard_map/all_gather | solution.py:78
  54.6 4.0 %multiply_reduce_fusion.1 = (f32[512,2]{0,1:T(2,128)}, f32[512,256]{0,1:T(8,128)}) fusion(bf16[512,2048]{1,0:T(8,128)(2,1)} %all-gather.4.cloned.1.call-done, bf16[2048,256]{1,0:T(8,128)(2,1)} %param.19), kind=kOutput, calls=%fused_computation.57 | convolution fusion | flops 537132032 | bytes 3674112 | tf_op jit(solution)/shard_map/dot_general | solution.py:82
  58.6 1.3 copy.80
  60.5 0.9 multiply_multiply_fusion.1
  61.4 1.5 subtract_convert_fusion.1
  62.9 1.1 pad_maximum_fusion.1
  64.8 3.3 %convolution_convert_fusion.1 = bf16[512,256]{0,1:T(8,128)(2,1)} fusion(bf16[512,2048]{1,0:T(8,128)(2,1)} %all-gather.4.cloned.1.call-done, bf16[2048,256]{1,0:T(8,128)(2,1)} %param.20), kind=kOutput, calls=%fused_computation.32 | convolution fusion | flops 537001984 | bytes 3407872 | tf_op jit(solution)/shard_map/dot_general | solution.py:83
  68.1 1.8 copy.85
  70.0 1.2 add_rsqrt_fusion.4
  71.2 1.6 fusion.39
  72.9 0.9 reshape.233
  74.0 1.6 fusion.24
  75.6 0.9 fusion.37
  76.5 31.9 %all_gather.20 = bf16[512,2,128]{2,0,1:T(8,128)(2,1)S(1)} all-gather(bf16[64,2,128]{2,0,1:T(8,128)(2,1)S(1)} %fusion.37), channel_id=1, replica_groups=mesh['sp'=8,'tp'=4] {'sp'}, dimensions={0}, use_global_device_ids=true | all-gather | bytes 294912 | tf_op jit(solution)/shard_map/all_gather | solution.py:105
  108.4 33.7 %all_gather.21 = bf16[512,2,128]{2,0,1:T(8,128)(2,1)} all-gather(bf16[64,2,128]{2,0,1:T(8,128)(2,1)S(1)} %bitcast.103), channel_id=1, replica_groups=mesh['sp'=8,'tp'=4] {'sp'}, dimensions={0}, use_global_device_ids=true | all-gather | bytes 294912 | tf_op jit(solution)/shard_map/all_gather | solution.py:106
  142.1 3.6 %multiply_reduce_fusion = (f32[512,4]{0,1:T(4,128)S(1)}, f32[512,512]{0,1:T(8,128)S(1)}) fusion(bf16[512,2048]{1,0:T(8,128)(2,1)} %all-gather.4.cloned.1.call-done, bf16[2048,512]{1,0:T(8,128)(2,1)} %param.18), kind=kOutput, calls=%fused_computation.44 | convolution fusion | flops 1074264064 | bytes 5251072 | tf_op jit(solution)/shard_map/dot_general | solution.py:81
  145.9 0.9 subtract_convert_fusion.3
  147.0 1.2 copy.73
  148.2 1.9 copy.74
  150.1 1.9 copy.75
  152.0 1.9 pad_maximum_fusion
  155.5 0.8 fusion.18
  156.3 1.2 fusion.19
  157.6 9.3 %all-gather.8.cloned.1.call-done = bf16[4096,2,128]{2,0,1:T(8,128)(2,1)} async-done(((bf16[512,2,128]{2,0,1:T(8,128)(2,1)}), bf16[4096,2,128]{2,0,1:T(8,128)(2,1)}) %all-gather.8.cloned.1.call-update) | async-done | bytes 2097168 | tf_op jit(solution)/shard_map/all_gather | solution.py:150
  166.9 52.2 %while.14 = (s32[]{:T(128)}, f32[2,1024]{1,0:T(2,128)S(1)}, f32[2,1024]{1,0:T(2,128)S(1)}, f32[2,1024,128]{2,1,0:T(8,128)S(1)}, bf16[2,2048,2,128]{3,1,0,2:T(8,1...) while((s32[]{:T(128)}, f32[2,1024]{1,0:T(2,128)S(1)}, ...), condition=%wide.region_10.11_spmd, body=%wide.region_7.10_spmd.sunk | while | flops 2181566464 | bytes 55182420 | solution.py:160
  166.9 9.4 %bitcast_reduce_fusion.2 = (f32[2,1024]{1,0:T(2,128)S(1)}, f32[2,2048,1024]{2,1,0:T(8,128)}) fusion(bf16[2,1024,128]{2,1,0:T(8,128)(2,1)} %get-tuple-element.194, bf16[2,2048,2,128]{3,1,0,2:T(8,128)(2,1)} %get-tuple-element.193, s32[]{:T(128)} %get-tuple-element.181), kind=kOutput, calls=%fused_computation.1.clone.1 | convolution fusion | flops 1082128384 | bytes 18358784 | tf_op jit(solution)/shard_map/while/body/eval_jaxpr/hqd,khd->hqk/dot_general | solution.py:135
  176.3 8.5 %fusion.80 = f32[2,1024]{1,0:T(2,128)S(1)} fusion(f32[2,2048,1024]{2,1,0:T(8,128)} %get-tuple-element.170, f32[2,1024]{1,0:T(2,128)S(1)} %max.4), kind=kLoop, calls=%fused_computation.4.clone.1 | loop fusion | flops 12580864 | bytes 16793600 | tf_op jit(solution)/shard_map/while/body/eval_jaxpr/reduce_sum | solution.py:147
  184.8 8.1 %fusion.81 = f32[2,1024,128]{2,1,0:T(8,128)S(1)} fusion(f32[2,2048,1024]{2,1,0:T(8,128)} %get-tuple-element.170, f32[2,1024]{1,0:T(2,128)S(1)} %max.4, bf16[2,2048,2,128]{3,1,0,2:T(8,128)(2,1)} %get-tuple-element.195, s32[]{:T(128)} %get-tuple-element.181, f32[2,1024,128]{2,1,0:T(8,128)S(1)} %get-tuple-element.184, f32[2,1024]{1,0:T(2,128)S(1)} %get-tuple-element.172), kind=kOutput, calls=%fused_computation.6.clone.1 | convolution fusion | flops 1086849024 | bytes 19939840 | tf_op jit(solution)/shard_map/while/body/eval_jaxpr/hqk,khd->hqd/dot_general | solution.py:141
  193.0 9.4 %bitcast_reduce_fusion.2 = (f32[2,1024]{1,0:T(2,128)S(1)}, f32[2,2048,1024]{2,1,0:T(8,128)}) fusion(bf16[2,1024,128]{2,1,0:T(8,128)(2,1)} %get-tuple-element.194, bf16[2,2048,2,128]{3,1,0,2:T(8,128)(2,1)} %get-tuple-element.193, s32[]{:T(128)} %get-tuple-element.181), kind=kOutput, calls=%fused_computation.1.clone.1 | convolution fusion | flops 1082128384 | bytes 18358784 | tf_op jit(solution)/shard_map/while/body/eval_jaxpr/hqd,khd->hqk/dot_general | solution.py:135
  202.4 8.5 %fusion.80 = f32[2,1024]{1,0:T(2,128)S(1)} fusion(f32[2,2048,1024]{2,1,0:T(8,128)} %get-tuple-element.170, f32[2,1024]{1,0:T(2,128)S(1)} %max.4), kind=kLoop, calls=%fused_computation.4.clone.1 | loop fusion | flops 12580864 | bytes 16793600 | tf_op jit(solution)/shard_map/while/body/eval_jaxpr/reduce_sum | solution.py:147
  210.9 8.1 %fusion.81 = f32[2,1024,128]{2,1,0:T(8,128)S(1)} fusion(f32[2,2048,1024]{2,1,0:T(8,128)} %get-tuple-element.170, f32[2,1024]{1,0:T(2,128)S(1)} %max.4, bf16[2,2048,2,128]{3,1,0,2:T(8,128)(2,1)} %get-tuple-element.195, s32[]{:T(128)} %get-tuple-element.181, f32[2,1024,128]{2,1,0:T(8,128)S(1)} %get-tuple-element.184, f32[2,1024]{1,0:T(2,128)S(1)} %get-tuple-element.172), kind=kOutput, calls=%fused_computation.6.clone.1 | convolution fusion | flops 1086849024 | bytes 19939840 | tf_op jit(solution)/shard_map/while/body/eval_jaxpr/hqk,khd->hqd/dot_general | solution.py:141
  219.1 1.1 divide_convert_fusion
  220.2 1.2 copy.88
  221.5 2.6 convolution_convert_fusion
  224.1 29.8 %reduce-scatter.2.cloned.1.call-done = bf16[128,2048]{1,0:T(8,128)(2,1)} async-done(((bf16[512,2048]{1,0:T(8,128)(2,1)}), bf16[128,2048]{1,0:T(8,128)(2,1)}) %reduce-scatter.2.cloned.1.call-update) | async-done | bytes 524304 | tf_op jit(solution)/shard_map/reduce_scatter | solution.py:168
  254.0 1.2 fusion.25
  255.2 2.1 fusion.31
  (61 shorter events, 5.9 us)
Async XLA Ops:
  6.5 214.9 %copy-start = (bf16[512,2048]{1,0:T(8,128)(2,1)S(1)}, bf16[512,2048]{1,0:T(8,128)(2,1)}, u32[]{:S(2)}) copy-start(bf16[512,2048]{1,0:T(8,128)(2,1)} %param.21) | copy-start | bytes 6291460
  6.5 48.0 %all-gather.4.cloned.1.call-start = ((), (), s32[]{:S(2)}) async-start(), calls=%async_computation.1 | async-start | bytes 2621440 | tf_op jit(solution)/shard_map/all_gather | solution.py:78
  9.0 4.7 %collective-permute-start = (f32[2,1536]{1,0:T(2,128)S(1)}, f32[2,1536]{1,0:T(2,128)S(1)}, u32[]{:S(2)}, u32[]{:S(2)}) collective-permute-start(f32[2,1536]{1,0:T(2,128)S(1)} %fusion.41), channel_id=1, source_target_pairs={{0,4},{4,0},{8,12},{12,8},{16,20},{20,16},{24,28},{28,24},{1,5},{5... | collective-permute-start | bytes 36872 | tf_op jit(solution)/shard_map/ppermute | solution.py:71
  13.7 3.8 %collective-permute-start.1 = (f32[2,1536]{1,0:T(2,128)S(1)}, f32[2,1536]{1,0:T(2,128)S(1)}, u32[]{:S(2)}, u32[]{:S(2)}) collective-permute-start(f32[2,1536]{1,0:T(2,128)S(1)} %add.164), channel_id=1, source_target_pairs={{0,8},{4,12},{8,0},{12,4},{16,24},{20,28},{24,16},{28,20},{1,9},{5... | collective-permute-start | bytes 36872 | tf_op jit(solution)/shard_map/ppermute | solution.py:71
  17.5 4.8 %collective-permute-start.2 = (f32[2,1536]{1,0:T(2,128)S(1)}, f32[2,1536]{1,0:T(2,128)S(1)}, u32[]{:S(2)}, u32[]{:S(2)}) collective-permute-start(f32[2,1536]{1,0:T(2,128)S(1)} %add.165), channel_id=1, source_target_pairs={{0,16},{4,20},{8,24},{12,28},{16,0},{20,4},{24,8},{28,12},{1,17},{... | collective-permute-start | bytes 36872 | tf_op jit(solution)/shard_map/ppermute | solution.py:71
  30.2 127.3 %all-gather.6.cloned.1.call-start = ((), (), s32[]{:S(2)}) async-start(), calls=%async_computation.2 | async-start | bytes 2359296 | tf_op jit(solution)/shard_map/all_gather | solution.py:149
  30.8 23.7 %copy-start.6 = (f32[512,32]{0,1:T(8,128)}, f32[512,32]{0,1:T(8,128)S(1)}, u32[]{:S(2)}) copy-start(f32[512,32]{0,1:T(8,128)S(1)} %get-tuple-element.112) | copy-start | bytes 196612
  30.9 23.7 %copy-start.8 = (f32[512,32]{0,1:T(8,128)}, f32[512,32]{0,1:T(8,128)S(1)}, u32[]{:S(2)}) copy-start(f32[512,32]{0,1:T(8,128)S(1)} %get-tuple-element.113) | copy-start | bytes 196612
  58.6 5.5 %copy-start.3 = (bf16[64,2048]{1,0:T(8,128)(2,1)S(1)}, bf16[64,2048]{1,0:T(8,128)(2,1)}, u32[]{:S(2)}) copy-start(bf16[64,2048]{1,0:T(8,128)(2,1)} %param.14) | copy-start | bytes 786436
  62.9 8.3 %copy-start.4 = (bf16[2048,256]{1,0:T(8,128)(2,1)S(1)}, bf16[2048,256]{1,0:T(8,128)(2,1)}, u32[]{:S(2)}) copy-start(bf16[2048,256]{1,0:T(8,128)(2,1)} %param.19) | copy-start | bytes 3145732
  64.0 102.9 %all-gather.8.cloned.1.call-start = ((), (), s32[]{:S(2)}) async-start(), calls=%async_computation.3 | async-start | bytes 2359296 | tf_op jit(solution)/shard_map/all_gather | solution.py:150
  69.9 184.0 %reduce-scatter.2.cloned.1.call-start = ((), (), s32[]{:S(2)}) async-start(), calls=%async_computation.4 | async-start | bytes 2621440 | tf_op jit(solution)/shard_map/reduce_scatter | solution.py:168
  142.0 3.6 %copy-start.11 = (f32[128]{0:T(128)S(1)}, f32[128]{0:T(128)}, u32[]{:S(2)}) copy-start(f32[128]{0:T(128)} %param.22) | copy-start | bytes 1540
  142.0 3.8 %copy-start.7 = (f32[512,32]{0,1:T(8,128)S(1)}, f32[512,32]{0,1:T(8,128)}, u32[]{:S(2)}) copy-start(f32[512,32]{0,1:T(8,128)} %copy-done.6) | copy-start | bytes 196612
  142.0 3.8 %copy-start.9 = (f32[512,32]{0,1:T(8,128)S(1)}, f32[512,32]{0,1:T(8,128)}, u32[]{:S(2)}) copy-start(f32[512,32]{0,1:T(8,128)} %copy-done.8) | copy-start | bytes 196612
  153.9 0.8 copy-start.1
  154.7 1.6 copy-start.5
  221.5 33.7 %copy-start.2 = (bf16[128,2048]{1,0:T(8,128)(2,1)S(1)}, bf16[128,2048]{1,0:T(8,128)(2,1)}, u32[]{:S(2)}) copy-start(bf16[128,2048]{1,0:T(8,128)(2,1)} %param.13) | copy-start | bytes 1572868
  221.5 33.7 %copy-start.10 = (f32[1,2048]{1,0:T(1,128)S(1)}, f32[1,2048]{1,0:T(1,128)}, u32[]{:S(2)}) copy-start(f32[1,2048]{1,0:T(1,128)} %get-tuple-element.103) | copy-start | bytes 24580
Sparse Core Ops, SparseCore 0:
  30.3 24.1 all-gather.3
  64.1 52.6 all-gather.5
  119.1 47.7 all-gather.7
  224.3 29.6 reduce-scatter.1
